TPU v7x, 512 devices: a 8x2x16 block of a 8x16x16 slice. The times are simulated.
512 devices in a mesh: grp: 2 (over y), fs: 16 (over z), tp: 16 (over x, core).
Axes of the slice: x: 8, y: 2, z: 16, core: 2. Of those that a mesh axis runs over, the one named last changes fastest.
The devices are a block of a 8x16x16 slice.
Arguments:
- tokens: bfloat16 [4096, 2048], P(('grp', 'fs'), 'tp'), parts along dimension 0, may hold values from -40 to 40
- norm_gain: float32 [2048], P('tp'), may hold values from 0.1 to 1.9
- expert_ids: int32 [4096, 8], P(('grp', 'fs')), parts along dimension 0, may hold values from 0 to 63, all different within a row; in each aligned block of 128 rows (0 to 127, 128 to 255, ...) at most 24 rows name the same one
- route_scores: float32 [4096, 8], P(('grp', 'fs')), parts along dimension 0, may hold values from 0.1 to 1
- gate_weight: float32 [64, 512, 2048], P(None, 'fs', 'tp'), may hold values from -0.125 to 0.125
- up_weight: float32 [64, 512, 2048], P(None, 'fs', 'tp'), may hold values from -0.125 to 0.125
- down_weight: float32 [64, 512, 2048], P(None, 'fs', 'tp'), may hold values from -0.25 to 0.25
- shared_gate: float32 [512, 2048], P('fs', 'tp'), may hold values from -0.125 to 0.125
- shared_up: float32 [512, 2048], P('fs', 'tp'), may hold values from -0.125 to 0.125
- shared_down: float32 [512, 2048], P('fs', 'tp'), may hold values from -0.25 to 0.25
Outputs:
- gate_served: bfloat16 [128, 512, 2048], P(('grp', 'fs'), None, 'tp'), parts along dimension 0
- up_served: bfloat16 [128, 512, 2048], P(('grp', 'fs'), None, 'tp'), parts along dimension 0
- down_served: bfloat16 [128, 512, 2048], P(('grp', 'fs'), None, 'tp'), parts along dimension 0
- shared_gate_served: bfloat16 [1024, 2048], P('grp', 'tp'), parts along dimension 0
- shared_up_served: bfloat16 [1024, 2048], P('grp', 'tp'), parts along dimension 0
- shared_down_served: bfloat16 [1024, 2048], P('grp', 'tp'), parts along dimension 0
- layer_output: bfloat16 [4096, 2048], P(('grp', 'fs'), 'tp'), parts along dimension 0
There are 2 independent parts, one for each index of `grp`. A program takes and returns all parts, laid end to end along the dimension named above; an argument that names none is the same for every part. Nothing has to cross between parts.
Inputs may be any that keep to these rules, and one draw needn't show every extreme that they name: `expert_ids`: each row names 8 different experts. Among the rows of one index of fs no expert is named more than 24 times; in every draw some expert reaches 24 on some index of fs.
All inputs are finite; a program needn't handle non-finite values.
Results may differ from a plain program's by a relative error of at most 0.03.
Values may be sent and summed in bfloat16 or wider, within the bound.
No kernel may reach another device: no remote copies, remote signals or barrier semaphores. Data moves between devices by JAX's collectives and lax.ppermute only.
A program may use at most 64 MiB of HBM per device.

v0:
```python
import jax
import jax.numpy as jnp
from jax import lax
from jax.sharding import Mesh
from jax.sharding import PartitionSpec as P

CAPACITY = 24
TP = ("tp_0", "tp_1")


norm_eps = 1e-05
routed_scale = 2.5


def copy_for_each(array, axis):
    size = lax.axis_size(axis)
    return lax.all_to_all(
        jnp.broadcast_to(array[None], (size, *array.shape)), axis, 0, 0, tiled=True
    )


def of_everyone(array, axis):
    return copy_for_each(array, axis).sum(axis=0)


def in_one(arrays, axis):
    ends = [0]
    for a in arrays:
        ends.append(ends[-1] + a.size)
    total = of_everyone(jnp.concatenate([a.ravel() for a in arrays]), axis)
    return tuple((total[b:e].reshape(a.shape) for a, b, e in zip(arrays, ends, ends[1:])))


def in_one_piece(arrays, axis, dim, along):
    both = jnp.concatenate(arrays, axis=along)
    result, at, finished = (lax.all_gather(both, axis, axis=dim, tiled=True), 0, [])
    for a in arrays:
        finished.append(lax.slice_in_dim(result, at, at + a.shape[along], axis=along))
        at += a.shape[along]
    return tuple(finished)


def side_by_side(arrays, axis, split_dim, concat_dim, along):
    both = jnp.concatenate(arrays, axis=along)
    result, at, finished = (
        lax.all_to_all(both, axis, split_axis=split_dim, concat_axis=concat_dim, tiled=True),
        0,
        [],
    )
    for a in arrays:
        finished.append(lax.slice_in_dim(result, at, at + a.shape[along], axis=along))
        at += a.shape[along]
    return tuple(finished)


def whole_of(array, axes, dim):
    for axis in reversed(axes):
        array = lax.all_gather(array, axis, axis=dim, tiled=True)
    return array


def on_device(
    tokens,
    norm_gain,
    expert_ids,
    route_scores,
    gate_weight,
    up_weight,
    down_weight,
    shared_gate,
    shared_up,
    shared_down,
):
    tok_float = tokens.astype(jnp.float32)
    row_sum, row_squares = in_one(
        (jnp.sum(tok_float, axis=1), jnp.sum(tok_float * tok_float, axis=1)), TP
    )
    full_width = tok_float.shape[1] * lax.axis_size(TP)
    row_mean = row_sum / full_width
    row_var = row_squares / full_width - row_mean * row_mean
    normed = ((tok_float - row_mean[:, None]) * lax.rsqrt(row_var + norm_eps)[:, None]).astype(
        jnp.bfloat16
    )
    gate_new = (gate_weight * norm_gain[None, None, :]).astype(jnp.bfloat16)
    up_new = (up_weight * norm_gain[None, None, :]).astype(jnp.bfloat16)
    down_new = down_weight.astype(jnp.bfloat16)
    gate_shared = (shared_gate * norm_gain[None, :]).astype(jnp.bfloat16)
    up_shared = (shared_up * norm_gain[None, :]).astype(jnp.bfloat16)
    down_shared = shared_down.astype(jnp.bfloat16)
    gate_whole, up_whole, down_whole = in_one_piece(
        (gate_shared, up_shared, down_shared), "fs", 0, 1
    )
    gate_local, up_local = side_by_side((gate_new, up_new), "fs", 0, 1, 2)
    shard_count = lax.axis_size("fs")
    experts_all = gate_weight.shape[0]
    experts_here = experts_all // shard_count
    tok_rows, top_count = expert_ids.shape
    slice_width = normed.shape[1]
    flat_ids = expert_ids.reshape(-1)
    one_hot = (flat_ids[:, None] == jnp.arange(experts_all, dtype=jnp.int32)[None, :]).astype(
        jnp.int32
    )
    earlier = jnp.sum((jnp.cumsum(one_hot, axis=0) - one_hot) * one_hot, axis=1)
    position = (
        flat_ids % experts_here * shard_count + flat_ids // experts_here
    ) * CAPACITY + earlier
    routed_rows = experts_all * CAPACITY
    source_row = (
        jnp.full((routed_rows,), tok_rows, jnp.int32)
        .at[position]
        .set(jnp.arange(flat_ids.shape[0], dtype=jnp.int32) // top_count)
    )
    padded = jnp.concatenate([normed, jnp.zeros((1, slice_width), jnp.bfloat16)], axis=0)
    outgoing = padded[source_row].reshape(experts_here, shard_count, CAPACITY, slice_width)
    arrived = lax.all_to_all(outgoing, "fs", split_axis=1, concat_axis=1, tiled=True)
    rows_in = arrived.reshape(experts_here, shard_count * CAPACITY, slice_width)
    paired = jnp.concatenate([gate_local, up_local], axis=1)
    hidden_width = paired.shape[1] // 2
    routed_terms = jnp.einsum("erd,efd->erf", rows_in, paired, preferred_element_type=jnp.float32)
    shared_pair = jnp.concatenate([gate_whole, up_whole], axis=0)
    shared_terms = lax.dot_general(
        normed, shared_pair, (((1,), (1,)), ((), ())), preferred_element_type=jnp.float32
    )
    all_terms = jnp.concatenate(
        [routed_terms.reshape(routed_rows, 2 * hidden_width), shared_terms], axis=0
    )
    down_local = lax.all_to_all(down_new, "fs", split_axis=0, concat_axis=1, tiled=True)
    row_share = lax.psum_scatter(
        all_terms.astype(jnp.bfloat16), TP, scatter_dimension=0, tiled=True
    ).astype(jnp.float32)
    hidden_part = (jax.nn.silu(row_share[:, :hidden_width]) * row_share[:, hidden_width:]).astype(
        jnp.bfloat16
    )
    hidden = whole_of(hidden_part, TP, 0)
    expert_hidden = hidden[:routed_rows].reshape(experts_here, shard_count * CAPACITY, hidden_width)
    outputs = jnp.einsum(
        "erf,efd->erd", expert_hidden, down_local, preferred_element_type=jnp.float32
    ).astype(jnp.bfloat16)
    returned = lax.all_to_all(
        outputs.reshape(experts_here, shard_count, CAPACITY, slice_width),
        "fs",
        split_axis=1,
        concat_axis=1,
        tiled=True,
    )
    returned = returned.reshape(routed_rows, slice_width)
    route_weight = route_scores / jnp.sum(route_scores, axis=1, keepdims=True) * routed_scale
    picked = returned[position].astype(jnp.float32) * route_weight.reshape(-1)[:, None]
    routed = jnp.sum(picked.reshape(tok_rows, top_count, slice_width), axis=1)
    shared_out = jnp.dot(hidden[routed_rows:], down_whole, preferred_element_type=jnp.float32)
    layer_out = (shared_out + routed).astype(jnp.bfloat16)
    return (gate_local, up_local, down_local, gate_whole, up_whole, down_whole, layer_out)


def solution(mesh):
    split = Mesh(
        mesh.devices.reshape(mesh.shape["grp"], mesh.shape["fs"], 8, 2),
        ("grp", "fs", "tp_0", "tp_1"),
    )
    return jax.shard_map(
        on_device,
        mesh=split,
        in_specs=(
            P(("grp", "fs"), TP),
            P(TP),
            P(("grp", "fs"), None),
            P(("grp", "fs"), None),
            P(None, "fs", TP),
            P(None, "fs", TP),
            P(None, "fs", TP),
            P("fs", TP),
            P("fs", TP),
            P("fs", TP),
        ),
        out_specs=(
            P(("grp", "fs"), None, TP),
            P(("grp", "fs"), None, TP),
            P(("grp", "fs"), None, TP),
            P("grp", TP),
            P("grp", TP),
            P("grp", TP),
            P(("grp", "fs"), TP),
        ),
        check_vma=False,
    )
```

profile of v0, /device:TPU:66, one launch (start us, length us, event | category | flops | bytes accessed | tf_op | source)
XLA Modules:
  0.0 359.0 jit_solution(13174853483276449634)
XLA Ops:
  7.2 0.9 convert_reduce_fusion
  8.1 0.6 broadcast_in_dim.6
  8.8 43.7 %all-to-all-start.2 = ((f32[16,1,256]{2,1,0:T(1,128)}), f32[16,1,256]{2,1,0:T(1,128)S(1)}, u32[]{:S(2)}, u32[]{:S(2)}) async-start(f32[16,1,256]{2,1,0:T(1,128)} %broadcast_in_dim.6), calls=%async_computation.2 | async-start | bytes 32768 | tf_op jit(solution)/shard_map/all_to_all | solution.py:17
  52.5 0.8 copy.55
  53.3 0.1 eq.31
  53.4 0.1 eq.27
  53.4 0.1 reshape.194
  53.6 18.0 %reduce-window.6 = s32[64,8,128]{2,1,0:T(8,128)S(1)} reduce-window(s32[64,8,128]{2,1,0:T(8,128)S(1)} %fusion.11, s32[]{:T(128)} %constant.59.clone.1), window={size=1x1x128 pad=0_0x0_0x127_0}, to_apply=%region_3.0 | reduce-window | flops 8323072 | bytes 524292 | tf_op jit(solution)/shard_map/reduce-window
  71.6 0.1 slice.61
  71.7 0.1 copy.58
  71.9 0.1 copy.59
  72.0 0.1 broadcast_add_fusion
  72.1 0.1 fusion.7
  72.3 4.3 %scatter_custom_fusion = s32[1536]{0:T(1024)S(1)} fusion(s32[1024]{0:T(1024)S(1)} %bitcast.56, s32[1024]{0:T(1024)S(1)} %add_select_fusion, s32[]{:T(128)} %constant.58.clone.1), kind=kCustom, calls=%fused_computation.57 | custom fusion | bytes 6148 | tf_op jit(solution)/shard_map/scatter | solution.py:111
  76.7 0.1 fusion.16
  76.8 0.6 copy-done.10
  77.4 3.2 gather_fusion
  80.6 0.8 copy.60
  81.4 7.7 %all-to-all-start.3 = ((bf16[4,16,24,128]{3,2,0,1:T(8,128)(2,1)}), bf16[4,16,24,128]{3,2,0,1:T(8,128)(2,1)S(1)}, u32[]{:S(2)}, u32[]{:S(2)}) async-start(bf16[4,16,24,128]{3,2,0,1:T(8,128)(2,1)} %copy.60), calls=%async_computation.3 | async-start | bytes 786432 | tf_op jit(solution)/shard_map/all_to_all | solution.py:115
  89.2 0.2 multiply_convert_fusion.1
  89.4 1.1 pad_maximum_fusion.1
  90.6 22.6 %all-to-all-done.3 = bf16[4,16,24,128]{3,2,0,1:T(8,128)(2,1)S(1)} async-done(((bf16[4,16,24,128]{3,2,0,1:T(8,128)(2,1)}), bf16[4,16,24,128]{3,2,0,1:T(8,128)(2,1)S(1)}, u32[]{:S(2)}, u32[]{:S(2)}) %all-to-all-start.3) | async-done | bytes 393248 | tf_op jit(solution)/shard_map/all_to_all | solution.py:115
  113.2 6.0 %all-to-all-start = ((bf16[64,32,256]{2,1,0:T(8,128)(2,1)}), bf16[64,32,256]{2,1,0:T(8,128)(2,1)S(1)}, u32[]{:S(2)}, u32[]{:S(2)}) async-start(bf16[64,32,256]{2,1,0:T(8,128)(2,1)} %pad_maximum_fusion.1), calls=%async_computation | async-start | bytes 2097152 | tf_op jit(solution)/shard_map/all_to_all | solution.py:46
  119.2 0.1 reduce-scatter.2.cloned.1.call-start
  119.3 73.0 %all_gather.9 = bf16[512,384]{1,0:T(8,128)(2,1)S(1)} all-gather(bf16[32,384]{1,0:T(8,128)(2,1)S(1)} %pad_maximum_fusion.2), channel_id=1, replica_groups=mesh['grp'=2,'fs'=16,'tp_0'=8,'tp_1'=2] {'fs'}, dimensions={0}, use_global_device_ids=true | all-gather | bytes 417792 | tf_op jit(solution)/shard_map/all_gather | solution.py:36
  192.4 0.1 fusion.27
  192.5 0.2 convolution_convert_fusion.2
  192.8 0.1 copy.52
  192.9 0.2 fusion.26
  193.1 1.0 convolution_convert_fusion
  194.1 2.0 pad_maximum_fusion
  196.3 0.1 all-gather.2.cloned.1.call-start
  196.3 65.2 %reduce-scatter.2.cloned.1.call-done = bf16[104,1024]{1,0:T(8,128)(2,1)} async-done(((bf16[1664,1024]{1,0:T(8,128)(2,1)}), bf16[104,1024]{1,0:T(8,128)(2,1)}) %reduce-scatter.2.cloned.1.call-update) | async-done | bytes 213008 | tf_op jit(solution)/shard_map/reduce_scatter | solution.py:128
  261.5 1.0 convert_element_type.61
  262.5 0.1 fusion.12
  262.6 2.1 all_gather.10
  264.8 0.1 convert_element_type.53
  264.9 41.8 %all_to_all.52 = bf16[64,32,128]{2,1,0:T(8,128)(2,1)S(1)} all-to-all(bf16[64,32,128]{2,1,0:T(8,128)(2,1)S(1)} %convert_element_type.53), channel_id=1, replica_groups=mesh['grp'=2,'fs'=16,'tp_0'=8,'tp_1'=2] {'fs'}, dimensions={0} | all-to-all | bytes 1048576 | tf_op jit(solution)/shard_map/all_to_all | solution.py:127
  306.7 6.7 %all-gather.2.cloned.1.call-done = bf16[1664,512]{1,0:T(8,128)(2,1)} async-done(((bf16[208,512]{1,0:T(8,128)(2,1)}), bf16[1664,512]{1,0:T(8,128)(2,1)}) %all-gather.2.cloned.1.call-update) | async-done | bytes 1703952 | tf_op jit(solution)/shard_map/all_gather | solution.py:58
  313.5 1.4 slice-done
  314.9 0.6 convolution_convert_fusion.1
  315.5 0.8 copy.62
  316.3 13.2 %all-to-all-start.4 = ((bf16[4,16,24,128]{3,2,0,1:T(8,128)(2,1)}), bf16[4,16,24,128]{3,2,0,1:T(8,128)(2,1)S(1)}, u32[]{:S(2)}, u32[]{:S(2)}) async-start(bf16[4,16,24,128]{3,2,0,1:T(8,128)(2,1)} %copy.62), calls=%async_computation.5 | async-start | bytes 786432 | tf_op jit(solution)/shard_map/all_to_all | solution.py:139
  329.5 0.1 copy.64
  329.6 18.2 %all-to-all-done.4 = bf16[4,16,24,128]{3,2,0,1:T(8,128)(2,1)S(1)} async-done(((bf16[4,16,24,128]{3,2,0,1:T(8,128)(2,1)}), bf16[4,16,24,128]{3,2,0,1:T(8,128)(2,1)S(1)}, u32[]{:S(2)}, u32[]{:S(2)}) %all-to-all-start.4) | async-done | bytes 393248 | tf_op jit(solution)/shard_map/all_to_all | solution.py:139
  347.8 3.2 gather_fusion.1
  351.1 0.2 fusion.4
  351.3 0.8 fusion
  (60 shorter events, 0.6 us)
Async XLA Ops:
  7.2 69.5 %copy-start.12 = (bf16[128,128]{1,0:T(8,128)(2,1)S(1)}, bf16[128,128]{1,0:T(8,128)(2,1)}, u32[]{:S(2)}) copy-start(bf16[128,128]{1,0:T(8,128)(2,1)} %param.10) | copy-start | bytes 98308
  8.8 67.9 %all-to-all-start.2 = ((f32[16,1,256]{2,1,0:T(1,128)}), f32[16,1,256]{2,1,0:T(1,128)S(1)}, u32[]{:S(2)}, u32[]{:S(2)}) async-start(f32[16,1,256]{2,1,0:T(1,128)} %broadcast_in_dim.6), calls=%async_computation.2 | async-start | bytes 32768 | tf_op jit(solution)/shard_map/all_to_all | solution.py:17
  76.8 0.6 copy-start.10
  77.4 11.7 %copy-start.4 = (f32[64,32,128]{2,1,0:T(8,128)S(1)}, f32[64,32,128]{2,1,0:T(8,128)}, u32[]{:S(2)}) copy-start(f32[64,32,128]{2,1,0:T(8,128)} %param.14) | copy-start | bytes 3145732
  77.4 11.7 %copy-start.5 = (f32[64,32,128]{2,1,0:T(8,128)S(1)}, f32[64,32,128]{2,1,0:T(8,128)}, u32[]{:S(2)}) copy-start(f32[64,32,128]{2,1,0:T(8,128)} %param.15) | copy-start | bytes 3145732
  77.4 11.7 %copy-start.17 = (f32[128]{0:T(128)S(1)}, f32[128]{0:T(128)}, u32[]{:S(2)}) copy-start(f32[128]{0:T(128)} %param.11) | copy-start | bytes 1540
  81.4 31.7 %all-to-all-start.3 = ((bf16[4,16,24,128]{3,2,0,1:T(8,128)(2,1)}), bf16[4,16,24,128]{3,2,0,1:T(8,128)(2,1)S(1)}, u32[]{:S(2)}, u32[]{:S(2)}) async-start(bf16[4,16,24,128]{3,2,0,1:T(8,128)(2,1)} %copy.60), calls=%async_computation.3 | async-start | bytes 786432 | tf_op jit(solution)/shard_map/all_to_all | solution.py:115
  89.4 29.9 %copy-start.15 = (f32[32,128]{1,0:T(8,128)S(1)}, f32[32,128]{1,0:T(8,128)}, u32[]{:S(2)}) copy-start(f32[32,128]{1,0:T(8,128)} %param.19) | copy-start | bytes 49156
  89.4 29.9 %copy-start.13 = (f32[32,128]{1,0:T(8,128)S(1)}, f32[32,128]{1,0:T(8,128)}, u32[]{:S(2)}) copy-start(f32[32,128]{1,0:T(8,128)} %param.17) | copy-start | bytes 49156
  89.4 29.9 %copy-start.14 = (f32[32,128]{1,0:T(8,128)S(1)}, f32[32,128]{1,0:T(8,128)}, u32[]{:S(2)}) copy-start(f32[32,128]{1,0:T(8,128)} %param.18) | copy-start | bytes 49156
  90.6 101.9 %copy-start.11 = (bf16[128,128]{1,0:T(8,128)(2,1)S(1)}, bf16[128,128]{1,0:T(8,128)(2,1)}, u32[]{:S(2)}) copy-start(bf16[128,128]{1,0:T(8,128)(2,1)} %copy-done.10) | copy-start | bytes 98308
  113.2 79.6 %all-to-all-start = ((bf16[64,32,256]{2,1,0:T(8,128)(2,1)}), bf16[64,32,256]{2,1,0:T(8,128)(2,1)S(1)}, u32[]{:S(2)}, u32[]{:S(2)}) async-start(bf16[64,32,256]{2,1,0:T(8,128)(2,1)} %pad_maximum_fusion.1), calls=%async_computation | async-start | bytes 2097152 | tf_op jit(solution)/shard_map/all_to_all | solution.py:46
  119.2 142.4 %reduce-scatter.2.cloned.1.call-start = ((), (), s32[]{:S(2)}) async-start(), calls=%async_computation.6 | async-start | bytes 3620864 | tf_op jit(solution)/shard_map/reduce_scatter | solution.py:128
  192.4 0.7 copy-start.7
  192.4 0.7 copy-start.8
  192.5 158.8 %copy-start.9 = (bf16[512,128]{1,0:T(8,128)(2,1)}, bf16[512,128]{1,0:T(8,128)(2,1)S(1)}, u32[]{:S(2)}) copy-start(bf16[512,128]{1,0:T(8,128)(2,1)S(1)} %get-tuple-element.11) | copy-start | bytes 393220
  193.1 1.0 copy-start
  193.1 1.0 copy-start.1
  196.2 68.6 %copy-start.3 = (f32[64,32,128]{2,1,0:T(8,128)S(1)}, f32[64,32,128]{2,1,0:T(8,128)}, u32[]{:S(2)}) copy-start(f32[64,32,128]{2,1,0:T(8,128)} %param.16) | copy-start | bytes 3145732
  196.3 117.2 %all-gather.2.cloned.1.call-start = ((), (), s32[]{:S(2)}) async-start(), calls=%async_computation.7 | async-start | bytes 1916928 | tf_op jit(solution)/shard_map/all_gather | solution.py:58
  306.7 8.7 %copy-start.6 = (bf16[16,4,32,128]{3,2,0,1:T(8,128)(2,1)}, bf16[16,4,32,128]{3,2,0,1:T(8,128)(2,1)S(1)}, u32[]{:S(2)}) copy-start(bf16[16,4,32,128]{3,2,0,1:T(8,128)(2,1)S(1)} %copy.53) | copy-start | bytes 1572868
  313.5 1.4 slice-start
  313.5 16.0 %copy-start.16 = (f32[128,8]{0,1:T(8,128)S(1)}, f32[128,8]{0,1:T(8,128)}, u32[]{:S(2)}) copy-start(f32[128,8]{0,1:T(8,128)} %param.13) | copy-start | bytes 12292
  316.3 35.0 %copy-start.2 = (bf16[1664,512]{1,0:T(8,128)(2,1)S(1)}, bf16[1664,512]{1,0:T(8,128)(2,1)}, u32[]{:S(2)}) copy-start(bf16[1664,512]{1,0:T(8,128)(2,1)} %all-gather.2.cloned.1.call-done) | copy-start | bytes 5111812
  316.3 31.5 %all-to-all-start.4 = ((bf16[4,16,24,128]{3,2,0,1:T(8,128)(2,1)}), bf16[4,16,24,128]{3,2,0,1:T(8,128)(2,1)S(1)}, u32[]{:S(2)}, u32[]{:S(2)}) async-start(bf16[4,16,24,128]{3,2,0,1:T(8,128)(2,1)} %copy.62), calls=%async_computation.5 | async-start | bytes 786432 | tf_op jit(solution)/shard_map/all_to_all | solution.py:139
Sparse Core Ops, SparseCore 0:
  196.4 65.1 reduce-scatter.1
  264.9 48.5 all-gather.1
where the time goes:
time: 360 us; the launch traced here: 359 us
  blocking collectives  117 us (32%)
  waiting for transfers between devices  113 us (31%)
  starting transfers between devices  70.8 us (20%)
  other arithmetic  24.2 us (7%)
  local copies, waits for them, and re-layouts  17.1 us (5%)
  between operations  14.6 us (4%)
    all_gather x1, blocking collectives, in_one_piece(): lax.all_gather(both, axis, axis=dim, tiled=True)  73 us
    reduce_scatter x1, waiting for transfers between devices, on_device(): lax.psum_scatter(all_terms.astype(jnp.bfloat16), TP, scatter_dimension=0,...  65.2 us
    all_to_all x1, starting transfers between devices, copy_for_each(): lax.all_to_all(jnp.broadcast_to(array[None], (size, *array.shape)), axis,...  43.7 us
    all_to_all x1, blocking collectives, on_device(): lax.all_to_all(down_new, 'fs', split_axis=0, concat_axis=1, tiled=True)  41.8 us
    all_to_all x1, waiting for transfers between devices, on_device(): lax.all_to_all(outgoing, 'fs', split_axis=1, concat_axis=1, tiled=True)  22.6 us
    another operation x3, other arithmetic  18.2 us
    all_to_all x1, waiting for transfers between devices, on_device(): lax.all_to_all(outputs.reshape(experts_here, shard_count, CAPACITY, slice...  18.2 us
    all_to_all x1, starting transfers between devices, on_device(): lax.all_to_all(outputs.reshape(experts_here, shard_count, CAPACITY, slice...  13.2 us
  transfers between devices with their start and end apart: 6, of which 4 were waited for; matrix products, arithmetic and copies ran while one was open for 7% of the time, Pallas kernels for 0%

commit v1 on v0

v1 whole, which is shorter than its diff:
```python
import jax
import jax.numpy as jnp
from jax import lax
from jax.sharding import Mesh
from jax.sharding import PartitionSpec as P

CAPACITY = 24
TP = ("tp_0", "tp_1")


norm_eps = 1e-05
routed_scale = 2.5


def exchange(array, axis):
    return lax.all_to_all(array, axis, 0, 0, tiled=True)


def copy_for_each(array, axis):
    size = lax.axis_size(axis)
    return exchange(jnp.broadcast_to(array[None], (size, *array.shape)), axis)


def swap_cores(array):
    return lax.ppermute(array, "tp_1", [(0, 1), (1, 0)])


def of_core(array, core, dim):
    half = array.shape[dim] // 2
    return lax.dynamic_slice_in_dim(array, core * half, half, axis=dim)


def with_shared(routed, shared, shards):
    experts, rows, width = routed.shape
    return jnp.concatenate(
        [
            routed.reshape(shards, experts // shards, rows, width),
            jnp.broadcast_to(shared[None, None], (shards, 1, rows, width)),
        ],
        axis=1,
    )


def by_expert(arrived):
    shards, experts, rows, width = arrived.shape
    return arrived.transpose(1, 0, 2, 3).reshape(experts, shards * rows, width)


def on_device(
    tokens,
    norm_gain,
    expert_ids,
    route_scores,
    gate_weight,
    up_weight,
    down_weight,
    shared_gate,
    shared_up,
    shared_down,
):
    shards = lax.axis_size("fs")
    chips = lax.axis_size("tp_0")
    core = lax.axis_index("tp_1")
    experts_all = gate_weight.shape[0]
    experts_here = experts_all // shards
    experts_core = experts_here // 2
    tok_rows, slice_width = tokens.shape
    tok_half = tok_rows // 2

    gain = norm_gain[None, None, :]
    gate_new = (gate_weight * gain).astype(jnp.bfloat16)
    up_new = (up_weight * gain).astype(jnp.bfloat16)
    down_new = down_weight.astype(jnp.bfloat16)
    gate_shared = (shared_gate * norm_gain[None, :]).astype(jnp.bfloat16)
    up_shared = (shared_up * norm_gain[None, :]).astype(jnp.bfloat16)
    down_shared = shared_down.astype(jnp.bfloat16)
    both_sent = jnp.stack(
        [with_shared(gate_new, gate_shared, shards), with_shared(up_new, up_shared, shards)], axis=1
    )
    both_here = exchange(both_sent, "fs")
    gate_all = by_expert(both_here[:, 0])
    up_all = by_expert(both_here[:, 1])

    tok_both = jnp.concatenate([tokens, swap_cores(tokens)], axis=1).astype(jnp.float32)
    sums = jnp.stack([jnp.sum(tok_both, axis=1), jnp.sum(tok_both * tok_both, axis=1)])
    row_sum, row_squares = copy_for_each(sums, "tp_0").sum(axis=0)
    full_width = slice_width * lax.axis_size(TP)
    row_mean = row_sum / full_width
    row_var = row_squares / full_width - row_mean * row_mean
    normed = ((tok_both - row_mean[:, None]) * lax.rsqrt(row_var + norm_eps)[:, None]).astype(
        jnp.bfloat16
    )

    route_weight = route_scores / jnp.sum(route_scores, axis=1, keepdims=True) * routed_scale
    named = expert_ids.T[:, None, :] == jnp.arange(experts_all, dtype=jnp.int32)[None, :, None]
    chosen = jnp.any(named, axis=0)
    weight_of = jnp.sum(jnp.where(named, route_weight.T[:, None, :], 0.0), axis=0)
    before = (
        jnp.arange(tok_rows, dtype=jnp.int32)[:, None] < jnp.arange(tok_rows, dtype=jnp.int32)[None, :]
    )
    rank = jnp.dot(
        chosen.astype(jnp.bfloat16), before.astype(jnp.bfloat16), preferred_element_type=jnp.float32
    )
    slot = jnp.where(chosen, rank.astype(jnp.int32), -1)
    slot = of_core(slot.reshape(shards, experts_here, tok_rows), core, 1)
    weight_of = of_core(weight_of.reshape(shards, experts_here, tok_rows), core, 1)
    in_slot = slot[:, :, None, :] == jnp.arange(CAPACITY, dtype=jnp.int32)[None, None, :, None]
    core_rows = shards * experts_core * CAPACITY
    select = in_slot.astype(jnp.bfloat16).reshape(core_rows, tok_rows)
    combine = jnp.where(in_slot, weight_of[:, :, None, :], 0.0).reshape(core_rows, tok_rows)

    outgoing = jnp.dot(select, normed, preferred_element_type=jnp.float32).astype(jnp.bfloat16)
    arrived = exchange(outgoing.reshape(shards, experts_core, CAPACITY, 2 * slice_width), "fs")
    rows_in = by_expert(arrived)

    hidden_width = gate_all.shape[1]
    paired = jnp.concatenate([gate_all, up_all], axis=1)

    def over_both(local, axis):
        mine = jnp.concatenate([of_core(local[:experts_here], core, 0), local[experts_here:]])
        theirs = jnp.concatenate([of_core(local[:experts_here], 1 - core, 0), local[experts_here:]])
        return jnp.concatenate([mine, swap_cores(theirs)], axis=axis)

    paired = over_both(paired, 2)
    routed_terms = jnp.einsum(
        "erd,efd->erf", rows_in, paired[:experts_core], preferred_element_type=jnp.float32
    ).astype(jnp.bfloat16)
    shared_terms = lax.dot_general(
        of_core(normed, core, 0),
        paired[experts_core],
        (((1,), (1,)), ((), ())),
        preferred_element_type=jnp.float32,
    ).astype(jnp.bfloat16)
    all_terms = jnp.concatenate(
        [routed_terms.reshape(core_rows, 2 * hidden_width), shared_terms], axis=0
    )
    part_rows = all_terms.shape[0] // chips
    parts = exchange(all_terms.reshape(chips, part_rows, 2 * hidden_width), "tp_0")
    row_share = jnp.sum(parts.astype(jnp.float32), axis=0)
    hidden_part = (jax.nn.silu(row_share[:, :hidden_width]) * row_share[:, hidden_width:]).astype(
        jnp.bfloat16
    )
    hidden = copy_for_each(hidden_part, "tp_0").reshape(chips * part_rows, hidden_width)

    down_all = by_expert(exchange(with_shared(down_new, down_shared, shards), "fs"))
    down_both = over_both(down_all, 2)
    outputs = jnp.einsum(
        "erf,efd->erd",
        hidden[:core_rows].reshape(experts_core, shards * CAPACITY, hidden_width),
        down_both[:experts_core],
        preferred_element_type=jnp.float32,
    ).astype(jnp.bfloat16)
    returned = exchange(
        outputs.reshape(experts_core, shards, CAPACITY, 2 * slice_width).transpose(1, 0, 2, 3), "fs"
    ).reshape(core_rows, 2 * slice_width)
    routed = lax.dot_general(
        combine,
        returned.astype(jnp.float32),
        (((0,), (0,)), ((), ())),
        precision=lax.Precision.HIGHEST,
        preferred_element_type=jnp.float32,
    )
    shared_out = jnp.dot(hidden[core_rows:], down_both[experts_core], preferred_element_type=jnp.float32)
    half_rows = jnp.arange(tok_rows, dtype=jnp.int32)[:, None] // tok_half == core
    total = routed + jnp.where(half_rows, jnp.concatenate([shared_out, shared_out], axis=0), 0.0)
    layer_out = (total[:, :slice_width] + swap_cores(total[:, slice_width:])).astype(jnp.bfloat16)
    return (
        gate_all[:experts_here],
        up_all[:experts_here],
        down_all[:experts_here],
        gate_all[experts_here],
        up_all[experts_here],
        down_all[experts_here],
        layer_out,
    )


def solution(mesh):
    split = Mesh(
        mesh.devices.reshape(mesh.shape["grp"], mesh.shape["fs"], mesh.shape["tp"] // 2, 2),
        ("grp", "fs", "tp_0", "tp_1"),
    )
    return jax.shard_map(
        on_device,
        mesh=split,
        in_specs=(
            P(("grp", "fs"), TP),
            P(TP),
            P(("grp", "fs"), None),
            P(("grp", "fs"), None),
            P(None, "fs", TP),
            P(None, "fs", TP),
            P(None, "fs", TP),
            P("fs", TP),
            P("fs", TP),
            P("fs", TP),
        ),
        out_specs=(
            P(("grp", "fs"), None, TP),
            P(("grp", "fs"), None, TP),
            P(("grp", "fs"), None, TP),
            P("grp", TP),
            P("grp", TP),
            P("grp", TP),
            P(("grp", "fs"), TP),
        ),
        check_vma=False,
    )
```

time: 360 us -> 316 us (0.88)
  the two profiles are of different devices: /device:TPU:66 before, /device:TPU:65 now
where the time goes in v1:
time: 316 us; the launch traced here: 315 us
  waiting for transfers between devices  163 us (52%)
  starting transfers between devices  126 us (40%)
  other arithmetic  11.2 us (4%)
  local copies, waits for them, and re-layouts  9.78 us (3%)
    all_to_all x7, waiting for transfers between devices, exchange(): return lax.all_to_all(array, axis, 0, 0, tiled=True)  162 us
    all_to_all x7, starting transfers between devices, exchange(): return lax.all_to_all(array, axis, 0, 0, tiled=True)  64.2 us
    ppermute x4, starting transfers between devices, swap_cores(): return lax.ppermute(array, 'tp_1', [(0, 1), (1, 0)])  62.3 us
  transfers between devices with their start and end apart: 11, of which 8 were waited for; matrix products, arithmetic and copies ran while one was open for 5% of the time, Pallas kernels for 0%

profile of v1, /device:TPU:65, one launch (start us, length us, event | category | flops | bytes accessed | tf_op | source)
XLA Modules:
  0.0 314.8 jit_solution(5600264288430108932)
XLA Ops:
  0.6 43.4 %collective-permute-start = (bf16[128,128]{1,0:T(8,128)(2,1)}, bf16[128,128]{1,0:T(8,128)(2,1)S(1)}, u32[]{:S(2)}, u32[]{:S(2)}) collective-permute-start(bf16[128,128]{1,0:T(8,128)(2,1)} %param.10), channel_id=1, source_target_pairs={{0,1},{1,0},{2,3},{3,2},{4,5},{5,4},{6,7},{7,6},{8,9},{9,8},{10,11... | collective-permute-start | bytes 98312 | tf_op jit(solution)/shard_map/ppermute | solution.py:25
  44.0 0.8 multiply_convert_fusion.3
  44.8 1.8 multiply_convert_fusion.1
  46.8 0.6 copy-done.3
  47.5 0.6 broadcast_in_dim.54
  48.1 3.5 %all-to-all-start.2 = ((f32[8,2,128]{2,1,0:T(2,128)}), f32[8,2,128]{2,1,0:T(2,128)S(1)}, u32[]{:S(2)}, u32[]{:S(2)}) async-start(f32[8,2,128]{2,1,0:T(2,128)} %broadcast_in_dim.54), calls=%async_computation.2 | async-start | bytes 16384 | tf_op jit(solution)/shard_map/all_to_all | solution.py:16
  51.6 1.2 pad_maximum_fusion.2
  52.8 5.2 %all-to-all-done.2 = f32[8,2,128]{2,1,0:T(2,128)S(1)} async-done(((f32[8,2,128]{2,1,0:T(2,128)}), f32[8,2,128]{2,1,0:T(2,128)S(1)}, u32[]{:S(2)}, u32[]{:S(2)}) %all-to-all-start.2) | async-done | bytes 8224 | tf_op jit(solution)/shard_map/all_to_all | solution.py:16
  58.0 7.1 %all-to-all-start = ((bf16[16,2,5,32,128]{4,3,2,1,0:T(8,128)(2,1)}), bf16[16,2,5,32,128]{4,3,2,1,0:T(8,128)(2,1)S(1)}, u32[]{:S(2)}, u32[]{:S(2)}) async-start(bf16[16,2,5,32,128]{4,3,2,1,0:T(8,128)(2,1)} %pad_maximum_fusion.2), calls=%async_computation | async-start | bytes 2621440 | tf_op jit(solution)/shard_map/all_to_all | solution.py:16
  65.4 0.2 bitcast_compare_fusion
  65.8 1.0 convolution_convert_fusion.2
  66.8 55.7 %all-to-all-done = bf16[16,2,5,32,128]{4,3,2,1,0:T(8,128)(2,1)S(1)} async-done(((bf16[16,2,5,32,128]{4,3,2,1,0:T(8,128)(2,1)}), bf16[16,2,5,32,128]{4,3,2,1,0:T(8,128)(2,1)S(1)}, u32[]{:S(2)}, u32[]{:S(2)}) %all-to-all-start) | async-done | bytes 1310752 | tf_op jit(solution)/shard_map/all_to_all | solution.py:16
  122.5 11.9 %all-to-all-start.3 = ((bf16[16,2,24,256]{3,2,1,0:T(8,128)(2,1)}), bf16[16,2,24,256]{3,2,1,0:T(8,128)(2,1)S(1)}, u32[]{:S(2)}, u32[]{:S(2)}) async-start(bf16[16,2,24,256]{3,2,1,0:T(8,128)(2,1)} %bitcast.27), calls=%async_computation.3 | async-start | bytes 786432 | tf_op jit(solution)/shard_map/all_to_all | solution.py:16
  134.4 0.2 fusion.33
  134.9 1.0 pad_maximum_fusion.3
  135.9 2.7 collective-permute-start.1
  138.6 13.3 %all-to-all-done.3 = bf16[16,2,24,256]{3,2,1,0:T(8,128)(2,1)S(1)} async-done(((bf16[16,2,24,256]{3,2,1,0:T(8,128)(2,1)}), bf16[16,2,24,256]{3,2,1,0:T(8,128)(2,1)S(1)}, u32[]{:S(2)}, u32[]{:S(2)}) %all-to-all-start.3) | async-done | bytes 393248 | tf_op jit(solution)/shard_map/all_to_all | solution.py:16
  151.9 0.2 pad_maximum_fusion.1
  152.1 0.6 convolution_convert_fusion
  152.7 0.3 convolution_convert_fusion.3
  153.0 1.4 pad_maximum_fusion
  154.3 3.9 %all-to-all-start.4 = ((bf16[8,104,1024]{2,1,0:T(8,128)(2,1)}), bf16[8,104,1024]{2,1,0:T(8,128)(2,1)S(1)}, u32[]{:S(2)}, u32[]{:S(2)}) async-start(bf16[8,104,1024]{2,1,0:T(8,128)(2,1)} %bitcast.83), calls=%async_computation.4 | async-start | bytes 3407872 | tf_op jit(solution)/shard_map/all_to_all | solution.py:16
  158.3 1.3 convert_element_type.56
  159.6 0.9 pad_maximum_fusion.5
  160.5 35.3 %all-to-all-done.4 = bf16[8,104,1024]{2,1,0:T(8,128)(2,1)S(1)} async-done(((bf16[8,104,1024]{2,1,0:T(8,128)(2,1)}), bf16[8,104,1024]{2,1,0:T(8,128)(2,1)S(1)}, u32[]{:S(2)}, u32[]{:S(2)}) %all-to-all-start.4) | async-done | bytes 1703968 | tf_op jit(solution)/shard_map/all_to_all | solution.py:16
  195.8 17.7 %all-to-all-start.1 = ((bf16[16,5,32,128]{3,2,1,0:T(8,128)(2,1)}), bf16[16,5,32,128]{3,2,1,0:T(8,128)(2,1)}, u32[]{:S(2)}, u32[]{:S(2)}) async-start(bf16[16,5,32,128]{3,2,1,0:T(8,128)(2,1)} %pad_maximum_fusion.5), calls=%async_computation.1 | async-start | bytes 1310720 | tf_op jit(solution)/shard_map/all_to_all | solution.py:16
  213.5 0.3 convert_reduce_fusion
  213.9 28.4 %all-to-all-done.1 = bf16[16,5,32,128]{3,2,1,0:T(8,128)(2,1)} async-done(((bf16[16,5,32,128]{3,2,1,0:T(8,128)(2,1)}), bf16[16,5,32,128]{3,2,1,0:T(8,128)(2,1)}, u32[]{:S(2)}, u32[]{:S(2)}) %all-to-all-start.1) | async-done | bytes 655392 | tf_op jit(solution)/shard_map/all_to_all | solution.py:16
  242.3 1.0 broadcast_in_dim.55
  243.3 3.8 %all-to-all-start.5 = ((bf16[8,104,512]{2,1,0:T(8,128)(2,1)}), bf16[8,104,512]{2,1,0:T(8,128)(2,1)S(1)}, u32[]{:S(2)}, u32[]{:S(2)}) async-start(bf16[8,104,512]{2,1,0:T(8,128)(2,1)} %broadcast_in_dim.55), calls=%async_computation.5 | async-start | bytes 1703936 | tf_op jit(solution)/shard_map/all_to_all | solution.py:16
  247.1 1.1 slice.108
  248.2 0.9 slice.111
  249.2 7.7 %collective-permute-start.2 = (bf16[3,512,128]{2,1,0:T(8,128)(2,1)S(1)}, bf16[3,512,128]{2,1,0:T(8,128)(2,1)S(1)}, u32[]{:S(2)}, u32[]{:S(2)}) collective-permute-start(bf16[3,512,128]{2,1,0:T(8,128)(2,1)S(1)} %pad_maximum_fusion.6), channel_id=1, source_target_pairs={{0,1},{1,0},{2,3},{3,2},{4,5},{5,4},{6,7},{7,6},{8,9},{9,8},{10,11... | collective-permute-start | bytes 1179656 | tf_op jit(solution)/shard_map/ppermute | solution.py:25
  256.9 1.3 collective-permute-done.2
  258.2 1.0 pad_maximum_fusion.4
  259.3 6.8 %all-to-all-done.5 = bf16[8,104,512]{2,1,0:T(8,128)(2,1)S(1)} async-done(((bf16[8,104,512]{2,1,0:T(8,128)(2,1)}), bf16[8,104,512]{2,1,0:T(8,128)(2,1)S(1)}, u32[]{:S(2)}, u32[]{:S(2)}) %all-to-all-start.5) | async-done | bytes 852000 | tf_op jit(solution)/shard_map/all_to_all | solution.py:16
  266.1 1.1 copy-done.2
  267.2 0.4 convolution_convert_fusion.1
  267.6 0.8 copy.54
  268.4 16.2 %all-to-all-start.6 = ((bf16[16,2,24,256]{3,2,1,0:T(8,128)(2,1)}), bf16[16,2,24,256]{3,2,1,0:T(8,128)(2,1)S(1)}, u32[]{:S(2)}, u32[]{:S(2)}) async-start(bf16[16,2,24,256]{3,2,1,0:T(8,128)(2,1)} %bitcast.74), calls=%async_computation.6 | async-start | bytes 786432 | tf_op jit(solution)/shard_map/all_to_all | solution.py:16
  284.9 17.2 %all-to-all-done.6 = bf16[16,2,24,256]{3,2,1,0:T(8,128)(2,1)S(1)} async-done(((bf16[16,2,24,256]{3,2,1,0:T(8,128)(2,1)}), bf16[16,2,24,256]{3,2,1,0:T(8,128)(2,1)S(1)}, u32[]{:S(2)}, u32[]{:S(2)}) %all-to-all-start.6) | async-done | bytes 393248 | tf_op jit(solution)/shard_map/all_to_all | solution.py:16
  302.1 0.5 fusion
  302.6 8.6 %collective-permute-start.3 = (f32[128,128]{1,0:T(8,128)S(1)}, f32[128,128]{1,0:T(8,128)S(1)}, u32[]{:S(2)}, u32[]{:S(2)}) collective-permute-start(f32[128,128]{1,0:T(8,128)S(1)} %slice.121), channel_id=1, source_target_pairs={{0,1},{1,0},{2,3},{3,2},{4,5},{5,4},{6,7},{7,6},{8,9},{9,8},{10,11... | collective-permute-start | bytes 196616 | tf_op jit(solution)/shard_map/ppermute | solution.py:25
  311.1 0.8 slice.105
  312.0 0.7 slice.109
  312.6 0.8 slice.107
  313.5 0.7 slice.110
  314.2 0.6 fusion.23
  (49 shorter events, 1.5 us)
Async XLA Ops:
  0.6 46.1 %collective-permute-start = (bf16[128,128]{1,0:T(8,128)(2,1)}, bf16[128,128]{1,0:T(8,128)(2,1)S(1)}, u32[]{:S(2)}, u32[]{:S(2)}) collective-permute-start(bf16[128,128]{1,0:T(8,128)(2,1)} %param.10), channel_id=1, source_target_pairs={{0,1},{1,0},{2,3},{3,2},{4,5},{5,4},{6,7},{7,6},{8,9},{9,8},{10,11... | collective-permute-start | bytes 98312 | tf_op jit(solution)/shard_map/ppermute | solution.py:25
  46.6 0.8 copy-start.3
  48.1 9.9 %all-to-all-start.2 = ((f32[8,2,128]{2,1,0:T(2,128)}), f32[8,2,128]{2,1,0:T(2,128)S(1)}, u32[]{:S(2)}, u32[]{:S(2)}) async-start(f32[8,2,128]{2,1,0:T(2,128)} %broadcast_in_dim.54), calls=%async_computation.2 | async-start | bytes 16384 | tf_op jit(solution)/shard_map/all_to_all | solution.py:16
  52.8 12.4 %copy-start.4 = (s32[128,8]{0,1:T(8,128)S(1)}, s32[128,8]{0,1:T(8,128)}, u32[]{:S(2)}) copy-start(s32[128,8]{0,1:T(8,128)} %param.12) | copy-start | bytes 12292
  58.0 64.5 %all-to-all-start = ((bf16[16,2,5,32,128]{4,3,2,1,0:T(8,128)(2,1)}), bf16[16,2,5,32,128]{4,3,2,1,0:T(8,128)(2,1)S(1)}, u32[]{:S(2)}, u32[]{:S(2)}) async-start(bf16[16,2,5,32,128]{4,3,2,1,0:T(8,128)(2,1)} %pad_maximum_fusion.2), calls=%async_computation | async-start | bytes 2621440 | tf_op jit(solution)/shard_map/all_to_all | solution.py:16
  122.5 29.4 %all-to-all-start.3 = ((bf16[16,2,24,256]{3,2,1,0:T(8,128)(2,1)}), bf16[16,2,24,256]{3,2,1,0:T(8,128)(2,1)S(1)}, u32[]{:S(2)}, u32[]{:S(2)}) async-start(bf16[16,2,24,256]{3,2,1,0:T(8,128)(2,1)} %bitcast.27), calls=%async_computation.3 | async-start | bytes 786432 | tf_op jit(solution)/shard_map/all_to_all | solution.py:16
  135.9 16.0 %collective-permute-start.1 = (bf16[3,1024,128]{2,1,0:T(8,128)(2,1)}, bf16[3,1024,128]{2,1,0:T(8,128)(2,1)S(1)}, u32[]{:S(2)}, u32[]{:S(2)}) collective-permute-start(bf16[3,1024,128]{2,1,0:T(8,128)(2,1)} %pad_maximum_fusion.3), channel_id=1, source_target_pairs={{0,1},{1,0},{2,3},{3,2},{4,5},{5,4},{6,7},{7,6},{8,9},{9,8},{10,11... | collective-permute-start | bytes 2359304 | tf_op jit(solution)/shard_map/ppermute | solution.py:25
  154.3 3.9 %copy-start.5 = (f32[32,128]{1,0:T(8,128)S(1)}, f32[32,128]{1,0:T(8,128)}, u32[]{:S(2)}) copy-start(f32[32,128]{1,0:T(8,128)} %param.19) | copy-start | bytes 49156
  154.3 41.5 %all-to-all-start.4 = ((bf16[8,104,1024]{2,1,0:T(8,128)(2,1)}), bf16[8,104,1024]{2,1,0:T(8,128)(2,1)S(1)}, u32[]{:S(2)}, u32[]{:S(2)}) async-start(bf16[8,104,1024]{2,1,0:T(8,128)(2,1)} %bitcast.83), calls=%async_computation.4 | async-start | bytes 3407872 | tf_op jit(solution)/shard_map/all_to_all | solution.py:16
  195.8 46.5 %all-to-all-start.1 = ((bf16[16,5,32,128]{3,2,1,0:T(8,128)(2,1)}), bf16[16,5,32,128]{3,2,1,0:T(8,128)(2,1)}, u32[]{:S(2)}, u32[]{:S(2)}) async-start(bf16[16,5,32,128]{3,2,1,0:T(8,128)(2,1)} %pad_maximum_fusion.5), calls=%async_computation.1 | async-start | bytes 1310720 | tf_op jit(solution)/shard_map/all_to_all | solution.py:16
  243.3 22.8 %all-to-all-start.5 = ((bf16[8,104,512]{2,1,0:T(8,128)(2,1)}), bf16[8,104,512]{2,1,0:T(8,128)(2,1)S(1)}, u32[]{:S(2)}, u32[]{:S(2)}) async-start(bf16[8,104,512]{2,1,0:T(8,128)(2,1)} %broadcast_in_dim.55), calls=%async_computation.5 | async-start | bytes 1703936 | tf_op jit(solution)/shard_map/all_to_all | solution.py:16
  249.1 35.6 %copy-start.1 = (bf16[1,16,32,128]{3,2,0,1:T(8,128)(2,1)}, bf16[1,16,32,128]{3,2,0,1:T(8,128)(2,1)S(1)}, u32[]{:S(2)}) copy-start(bf16[1,16,32,128]{3,2,0,1:T(8,128)(2,1)S(1)} %slice.111) | copy-start | bytes 393220
  249.1 10.1 %copy-start = (bf16[4,16,32,128]{3,2,1,0:T(8,128)(2,1)}, bf16[4,16,32,128]{3,2,1,0:T(8,128)(2,1)S(1)}, u32[]{:S(2)}) copy-start(bf16[4,16,32,128]{3,2,1,0:T(8,128)(2,1)S(1)} %copy.39) | copy-start | bytes 1572868
  249.2 9.0 %collective-permute-start.2 = (bf16[3,512,128]{2,1,0:T(8,128)(2,1)S(1)}, bf16[3,512,128]{2,1,0:T(8,128)(2,1)S(1)}, u32[]{:S(2)}, u32[]{:S(2)}) collective-permute-start(bf16[3,512,128]{2,1,0:T(8,128)(2,1)S(1)} %pad_maximum_fusion.6), channel_id=1, source_target_pairs={{0,1},{1,0},{2,3},{3,2},{4,5},{5,4},{6,7},{7,6},{8,9},{9,8},{10,11... | collective-permute-start | bytes 1179656 | tf_op jit(solution)/shard_map/ppermute | solution.py:25
  266.1 1.1 copy-start.2
  267.2 17.4 %copy-start.6 = (f32[128,8]{0,1:T(8,128)S(1)}, f32[128,8]{0,1:T(8,128)}, u32[]{:S(2)}) copy-start(f32[128,8]{0,1:T(8,128)} %param.13) | copy-start | bytes 12292
  268.4 33.7 %all-to-all-start.6 = ((bf16[16,2,24,256]{3,2,1,0:T(8,128)(2,1)}), bf16[16,2,24,256]{3,2,1,0:T(8,128)(2,1)S(1)}, u32[]{:S(2)}, u32[]{:S(2)}) async-start(bf16[16,2,24,256]{3,2,1,0:T(8,128)(2,1)} %bitcast.74), calls=%async_computation.6 | async-start | bytes 786432 | tf_op jit(solution)/shard_map/all_to_all | solution.py:16
  302.6 11.6 %collective-permute-start.3 = (f32[128,128]{1,0:T(8,128)S(1)}, f32[128,128]{1,0:T(8,128)S(1)}, u32[]{:S(2)}, u32[]{:S(2)}) collective-permute-start(f32[128,128]{1,0:T(8,128)S(1)} %slice.121), channel_id=1, source_target_pairs={{0,1},{1,0},{2,3},{3,2},{4,5},{5,4},{6,7},{7,6},{8,9},{9,8},{10,11... | collective-permute-start | bytes 196616 | tf_op jit(solution)/shard_map/ppermute | solution.py:25
